TPU v7x, 512 devices: a whole 4x8x8 slice. The times are simulated.
512 devices in a mesh: fs: 64 (over z, y), tp: 8 (over x, core).
Axes of the slice: x: 4, y: 8, z: 8, core: 2. Of those that a mesh axis runs over, the one named last changes fastest.
Arguments:
- tokens: bfloat16 [24576, 2048], P('fs', 'tp'), may hold values from -8 to 8
- w_value: bfloat16 [2048, 1024], P('fs', 'tp'), may hold values from -0.125 to 0.125
- w_gate: bfloat16 [2048, 1024], P('fs', 'tp'), may hold values from -0.125 to 0.125
- conv_kernel: bfloat16 [31, 1024], replicated, may hold values from -1 to 1
- conv_gain: float32 [1024], replicated, may hold values from 0.1 to 1.9
- w_mix_out: bfloat16 [1024, 2048], P('fs', 'tp'), may hold values from -0.1875 to 0.1875
- mix_gain: float32 [2048], replicated, may hold values from 0.1 to 1.9
- w_up: bfloat16 [2048, 8192], P('fs', 'tp'), may hold values from -0.125 to 0.125
- w_down: bfloat16 [8192, 2048], P('tp', 'fs'), may hold values from -0.0625 to 0.0625
- out_gain: float32 [2048], replicated, may hold values from 0.1 to 1.9
Outputs:
- result: bfloat16 [24576, 2048], P('fs', 'tp')
All inputs are finite; a program needn't handle non-finite values.
Results may differ from a plain program's by a relative error of at most 0.013.
Values may be sent and summed in bfloat16 or wider, within the bound.
No kernel may reach another device: no remote copies, remote signals or barrier semaphores. Data moves between devices by JAX's collectives and lax.ppermute only.
A program may use at most 64 MiB of HBM per device.

v0:
```python
import jax
import jax.numpy as jnp
from jax import lax
from jax.sharding import Mesh
from jax.sharding import PartitionSpec as P

WIDTH = 2048
CHANNELS = 1024
KERNEL = 31
LENGTH = 128
FS = ("fs_0", "fs_1")
norm_eps = 1e-05
residual_scale = 2.0**0.5


def joined_along(parts, dim):
    lengths = list(parts.shape[1:])
    lengths[dim] *= parts.shape[0]
    return jnp.moveaxis(parts, 0, dim).reshape(lengths)


def gather_in_order(shard, axes, order):
    parts = shard[None]
    for k in order:
        parts = lax.all_gather(parts, axes[k], axis=0, tiled=True)
    current = [lax.axis_size(axes[k]) for k in reversed(order)]
    parts = parts.reshape(*current, *shard.shape)
    turned = sorted(range(len(order)), key=lambda place: order[len(order) - 1 - place])
    return parts.transpose(*turned, *range(len(order), parts.ndim)).reshape(-1, *shard.shape)


def whole_of(shard, axes, order, dim):
    return joined_along(gather_in_order(shard, axes, order), dim)


def sent_to_all(shard, axis):
    copies = jnp.broadcast_to(shard, (lax.axis_size(axis), *shard.shape))
    return lax.all_to_all(copies, axis, split_axis=0, concat_axis=0, tiled=True)


def gather_directly(shard, axis, dim):
    return joined_along(sent_to_all(shard, axis), dim)


def in_one_piece(arrays, axis, dim, along):
    both = jnp.concatenate(arrays, axis=along)
    out, at, done = (lax.all_gather(both, axis, axis=dim, tiled=True), 0, [])
    for a in arrays:
        done.append(lax.slice_in_dim(out, at, at + a.shape[along], axis=along))
        at += a.shape[along]
    return tuple(done)


def taken_together(shard, axis):
    everything = sent_to_all(shard, axis)
    return jnp.sum(everything, axis=0)


def in_one(arrays, axis):
    ends = [0]
    for a in arrays:
        ends.append(ends[-1] + a.size)
    total = taken_together(jnp.concatenate([a.ravel() for a in arrays]), axis)
    return tuple((total[b:e].reshape(a.shape) for a, b, e in zip(arrays, ends, ends[1:])))


def in_blocks(shard, dim, count):
    lengths = shard.shape
    parts = shard.reshape(*lengths[:dim], count, lengths[dim] // count, *lengths[dim + 1 :])
    return jnp.moveaxis(parts, dim, 0)


def summed_on_arrival(shard, axis, dim):
    count = lax.axis_size(axis)
    parts = lax.all_to_all(in_blocks(shard, dim, count), axis, 0, 0, tiled=True)
    return jnp.sum(parts.astype(jnp.float32), axis=0)


def causal_filter(gated, kernel):
    sequences = gated.shape[0] // LENGTH
    frames = gated.astype(jnp.float32).reshape(sequences, LENGTH, gated.shape[1])
    padded = jnp.pad(frames, ((0, 0), (KERNEL - 1, 0), (0, 0)))
    accumulated = jnp.zeros(frames.shape, jnp.float32)
    for offset in range(KERNEL):
        accumulated = (
            accumulated + kernel[offset].astype(jnp.float32) * padded[:, offset : offset + LENGTH]
        )
    return accumulated.reshape(gated.shape[0], gated.shape[1])


def normalize(values, total_sum, total_sq, entries, gain_vector):
    average = total_sum / entries
    spread = jnp.maximum(total_sq / entries - average * average, 0.0)
    return (values - average[:, None]) * lax.rsqrt(spread[:, None] + norm_eps) * gain_vector


def add_rows(piece, source):
    return jnp.dot(source, piece, preferred_element_type=jnp.float32)


def add_pair(pieces, source):
    first = jnp.dot(source, pieces[0], preferred_element_type=jnp.float32)
    second = jnp.dot(source, pieces[1], preferred_element_type=jnp.float32)
    return (first, second)


def per_device(
    tokens, w_value, w_gate, conv_kernel, conv_gain, w_mix_out, mix_gain, w_up, w_down, out_gain
):
    tp_rank = lax.axis_index("tp")
    width_part = tokens.shape[1]
    channel_part = w_value.shape[1]
    up_collected = lax.all_gather(w_up, FS, axis=0, tiled=True)
    down_collected = whole_of(w_down, FS, (0, 1), 1)
    features = gather_directly(tokens, "tp", 1)
    values_proj, gate_proj = add_pair(in_one_piece((w_value, w_gate), FS, 0, 1), source=features)
    gated = (values_proj * jax.nn.sigmoid(gate_proj)).astype(jnp.bfloat16)
    kernel = lax.dynamic_slice_in_dim(conv_kernel, tp_rank * channel_part, channel_part, 1)
    filtered = causal_filter(gated, kernel)
    channel_sum, channel_sq = in_one((jnp.sum(filtered, 1), jnp.sum(filtered * filtered, 1)), "tp")
    channel_gain = lax.dynamic_slice_in_dim(conv_gain, tp_rank * channel_part, channel_part, 0)
    activated = jax.nn.silu(
        normalize(filtered, channel_sum, channel_sq, CHANNELS, channel_gain)
    ).astype(jnp.bfloat16)
    all_channels = gather_directly(activated, "tp", 1)
    mixed = add_rows(gather_directly(w_mix_out, FS, 0), source=all_channels)
    combined = residual_scale * tokens.astype(jnp.float32) + mixed
    middle_sum, middle_sq = in_one((jnp.sum(combined, 1), jnp.sum(combined * combined, 1)), "tp")
    middle_gain = lax.dynamic_slice_in_dim(mix_gain, tp_rank * width_part, width_part, 0)
    middle = normalize(combined, middle_sum, middle_sq, WIDTH, middle_gain).astype(jnp.bfloat16)
    middle_whole = gather_directly(middle, "tp", 1)
    up_proj = jnp.dot(middle_whole, up_collected, preferred_element_type=jnp.float32)
    hidden = jnp.square(jax.nn.relu(up_proj)).astype(jnp.bfloat16)
    terms = jnp.dot(hidden, down_collected, preferred_element_type=jnp.float32)
    down_sum = summed_on_arrival(terms.astype(jnp.bfloat16), "tp", 1)
    final = residual_scale * middle.astype(jnp.float32) + down_sum
    final_sum, final_sq = in_one((jnp.sum(final, 1), jnp.sum(final * final, 1)), "tp")
    final_gain = lax.dynamic_slice_in_dim(out_gain, tp_rank * width_part, width_part, 0)
    return normalize(final, final_sum, final_sq, WIDTH, final_gain).astype(jnp.bfloat16)


def solution(mesh):
    split = Mesh(mesh.devices.reshape(8, 8, mesh.shape["tp"]), ("fs_0", "fs_1", "tp"))
    in_specs = (
        P(FS, "tp"),
        P(FS, "tp"),
        P(FS, "tp"),
        P(),
        P(),
        P(FS, "tp"),
        P(),
        P(FS, "tp"),
        P("tp", FS),
        P(),
    )
    out_specs = P(FS, "tp")
    return jax.shard_map(
        per_device, mesh=split, in_specs=in_specs, out_specs=out_specs, check_vma=False
    )
```

profile of v0, /device:TPU:1, one launch (start us, length us, event | category | flops | bytes accessed | tf_op | source)
XLA Modules:
  0.0 304.4 jit_solution(7589131715608800212)
XLA Ops:
  6.5 0.0 copy-start.1
  6.5 0.0 all-gather.5.cloned.1.call-start
  6.5 1.4 pad_maximum_fusion
  7.9 0.0 all-gather.5.cloned.1.call-update
  7.9 0.0 all-gather.9.cloned.1.call-start
  8.0 27.1 %all-gather = bf16[8192,32]{0,1:T(8,128)(2,1)S(1)} all-gather(bf16[1024,32]{0,1:T(8,128)(2,1)} %param.18), channel_id=2, replica_groups=mesh['fs_0'=8,'fs_1'=8,'tp'=8] {'fs_0'}, dimensions={0}, use_global_device_ids=true | all-gather | bytes 589824 | tf_op jit(solution)/shard_map/all_gather | solution.py:25
  35.1 1.1 copy.78
  36.2 0.0 all-gather.9.cloned.1.call-update
  36.2 0.0 all-gather.7.cloned.1.call-start
  36.3 0.7 all-gather.7.cloned.1.call-update
  37.0 0.0 copy-done.1
  37.0 0.2 copy.53
  37.2 1.4 broadcast_in_dim.16
  38.5 10.5 %all-to-all-start = ((bf16[8,384,256]{1,2,0:T(8,128)(2,1)}), bf16[8,384,256]{1,2,0:T(8,128)(2,1)S(1)}, u32[]{:S(2)}, u32[]{:S(2)}) async-start(bf16[8,384,256]{1,2,0:T(8,128)(2,1)} %broadcast_in_dim.16), calls=%async_computation | async-start | bytes 3145728 | tf_op jit(solution)/shard_map/all_to_all | solution.py:38
  49.0 1.0 fusion.102
  50.1 1.1 fusion.103
  51.2 18.4 %all-to-all-done = bf16[8,384,256]{1,2,0:T(8,128)(2,1)S(1)} async-done(((bf16[8,384,256]{1,2,0:T(8,128)(2,1)}), bf16[8,384,256]{1,2,0:T(8,128)(2,1)S(1)}, u32[]{:S(2)}, u32[]{:S(2)}) %all-to-all-start) | async-done | bytes 1572896 | tf_op jit(solution)/shard_map/all_to_all | solution.py:38
  69.6 23.6 %all-gather.5.cloned.1.call-done = bf16[2048,256]{1,0:T(8,128)(2,1)} async-done(((bf16[32,256]{1,0:T(8,128)(2,1)}), bf16[2048,256]{1,0:T(8,128)(2,1)}) %all-gather.5.cloned.1.call-update) | async-done | bytes 1048592 | tf_op jit(solution)/shard_map/all_gather | solution.py:47
  93.2 0.0 copy-start
  93.2 1.6 fusion.8
  94.8 0.0 copy-done
  94.8 0.0 copy-start.2
  94.9 0.5 fusion.6
  95.4 0.1 copy.55
  95.5 0.7 fusion.106
  96.3 14.3 %all_to_all.43 = f32[8,1,768]{2,1,0:T(1,128)S(1)} all-to-all(f32[8,1,768]{2,1,0:T(1,128)S(1)} %broadcast_in_dim.17), channel_id=1, replica_groups=mesh['fs_0'=8,'fs_1'=8,'tp'=8] {'tp'}, dimensions={0} | all-to-all | bytes 49152 | tf_op jit(solution)/shard_map/all_to_all | solution.py:38
  110.5 0.0 copy-done.2
  110.5 0.9 broadcast_in_dim.19
  111.4 8.6 %all-to-all-start.3 = ((bf16[64,16,256]{2,1,0:T(8,128)(2,1)}), bf16[64,16,256]{2,1,0:T(8,128)(2,1)S(1)}, u32[]{:S(2)}, u32[]{:S(2)}) async-start(bf16[64,16,256]{2,1,0:T(8,128)(2,1)} %broadcast_in_dim.19), calls=%async_computation.3 | async-start | bytes 1048576 | tf_op jit(solution)/shard_map/all_to_all | solution.py:38
  120.0 0.8 dynamic_slice.13
  120.8 0.2 multiply_convert_fusion.3
  121.0 0.1 copy.57
  121.1 22.2 %all-to-all-done.3 = bf16[64,16,256]{2,1,0:T(8,128)(2,1)S(1)} async-done(((bf16[64,16,256]{2,1,0:T(8,128)(2,1)}), bf16[64,16,256]{2,1,0:T(8,128)(2,1)S(1)}, u32[]{:S(2)}, u32[]{:S(2)}) %all-to-all-start.3) | async-done | bytes 524320 | tf_op jit(solution)/shard_map/all_to_all | solution.py:38
  143.4 0.1 broadcast_in_dim.18
  143.5 16.5 %all_to_all.44 = bf16[8,384,128]{1,2,0:T(8,128)(2,1)S(1)} all-to-all(bf16[8,384,128]{1,2,0:T(8,128)(2,1)S(1)} %broadcast_in_dim.18), channel_id=1, replica_groups=mesh['fs_0'=8,'fs_1'=8,'tp'=8] {'tp'}, dimensions={0} | all-to-all | bytes 1572864 | tf_op jit(solution)/shard_map/all_to_all | solution.py:38
  159.9 0.5 fusion.105
  160.5 0.6 broadcast_in_dim.20
  161.1 4.2 %all-to-all-start.4 = ((f32[8,1,768]{2,1,0:T(1,128)}), f32[8,1,768]{2,1,0:T(1,128)S(1)}, u32[]{:S(2)}, u32[]{:S(2)}) async-start(f32[8,1,768]{2,1,0:T(1,128)} %broadcast_in_dim.20), calls=%async_computation.4 | async-start | bytes 49152 | tf_op jit(solution)/shard_map/all_to_all | solution.py:38
  165.3 0.8 dynamic_slice.14
  166.1 3.9 %all-to-all-done.4 = f32[8,1,768]{2,1,0:T(1,128)S(1)} async-done(((f32[8,1,768]{2,1,0:T(1,128)}), f32[8,1,768]{2,1,0:T(1,128)S(1)}, u32[]{:S(2)}, u32[]{:S(2)}) %all-to-all-start.4) | async-done | bytes 24608 | tf_op jit(solution)/shard_map/all_to_all | solution.py:38
  170.0 0.1 multiply_convert_fusion.2
  170.2 1.3 broadcast_in_dim.21
  171.5 4.2 %all-to-all-start.5 = ((bf16[8,384,256]{1,2,0:T(8,128)(2,1)}), bf16[8,384,256]{1,2,0:T(8,128)(2,1)S(1)}, u32[]{:S(2)}, u32[]{:S(2)}) async-start(bf16[8,384,256]{1,2,0:T(8,128)(2,1)} %broadcast_in_dim.21), calls=%async_computation.5 | async-start | bytes 3145728 | tf_op jit(solution)/shard_map/all_to_all | solution.py:38
  175.7 0.0 all-gather.9.cloned.1.call-done
  175.7 6.5 %copy.60 = bf16[8,8,1024,32]{2,3,1,0:T(8,128)(2,1)} copy(bf16[8,8,1024,32]{2,0,1,3:T(8,128)(2,1)} %bitcast.207) | data formatting | bytes 8388608 | tf_op jit(solution)/shard_map/transpose | solution.py:29
  182.2 14.1 %all-to-all-done.5 = bf16[8,384,256]{1,2,0:T(8,128)(2,1)S(1)} async-done(((bf16[8,384,256]{1,2,0:T(8,128)(2,1)}), bf16[8,384,256]{1,2,0:T(8,128)(2,1)S(1)}, u32[]{:S(2)}, u32[]{:S(2)}) %all-to-all-start.5) | async-done | bytes 1572896 | tf_op jit(solution)/shard_map/all_to_all | solution.py:38
  196.3 53.9 %all-gather.7.cloned.1.call-done = bf16[2048,1024]{1,0:T(8,128)(2,1)} async-done(((bf16[32,1024]{1,0:T(8,128)(2,1)}), bf16[2048,1024]{1,0:T(8,128)(2,1)}) %all-gather.7.cloned.1.call-update) | async-done | bytes 4194320 | tf_op jit(solution)/shard_map/all_gather | solution.py:113
  250.2 6.9 %convolution_convert_fusion = bf16[384,2048]{1,0:T(8,128)(2,1)S(1)} fusion(bf16[1024,2048]{0,1:T(8,128)(2,1)} %bitcast.208, bf16[384,2048]{0,1:T(8,128)(2,1)S(1)} %bitcast.211, bf16[2048,1024]{1,0:T(8,128)(2,1)} %all-gather.7.cloned.1.call-done), kind=kOutput, calls=%fused_computation.1 | convolution fusion | flops 3223191552 | bytes 11534336 | tf_op jit(solution)/shard_map/dot_general | solution.py:134
  257.1 0.1 copy.80
  257.2 29.4 %all_to_all.45 = bf16[8,384,256]{2,1,0:T(8,128)(2,1)S(1)} all-to-all(bf16[8,384,256]{2,1,0:T(8,128)(2,1)S(1)} %bitcast.206), channel_id=1, replica_groups=mesh['fs_0'=8,'fs_1'=8,'tp'=8] {'tp'}, dimensions={0} | all-to-all | bytes 3145728 | tf_op jit(solution)/shard_map/all_to_all | solution.py:75
  286.6 0.2 convert_reduce_fusion
  286.8 0.2 copy.63
  287.0 0.2 fusion.72
  287.2 0.6 broadcast_in_dim.23
  287.8 4.3 %all-to-all-start.7 = ((f32[8,1,768]{2,1,0:T(1,128)}), f32[8,1,768]{2,1,0:T(1,128)S(1)}, u32[]{:S(2)}, u32[]{:S(2)}) async-start(f32[8,1,768]{2,1,0:T(1,128)} %broadcast_in_dim.23), calls=%async_computation.7 | async-start | bytes 49152 | tf_op jit(solution)/shard_map/all_to_all | solution.py:38
  292.1 0.8 dynamic_slice.15
  292.9 3.9 %all-to-all-done.7 = f32[8,1,768]{2,1,0:T(1,128)S(1)} async-done(((f32[8,1,768]{2,1,0:T(1,128)}), f32[8,1,768]{2,1,0:T(1,128)S(1)}, u32[]{:S(2)}, u32[]{:S(2)}) %all-to-all-start.7) | async-done | bytes 24608 | tf_op jit(solution)/shard_map/all_to_all | solution.py:38
  296.8 0.2 multiply_convert_fusion.1
  297.0 0.8 copy.65
  (10 shorter events, 0.2 us)
Async XLA Ops:
  6.5 30.4 %copy-start.1 = (bf16[384,256]{1,0:T(8,128)(2,1)S(1)}, bf16[384,256]{1,0:T(8,128)(2,1)}, u32[]{:S(2)}) copy-start(bf16[384,256]{1,0:T(8,128)(2,1)} %param.10) | copy-start | bytes 589828
  6.5 86.7 %all-gather.5.cloned.1.call-start = ((), (), s32[]{:S(2)}) async-start(), calls=%async_computation.8 | async-start | bytes 1064960 | tf_op jit(solution)/shard_map/all_gather | solution.py:47
  7.9 167.8 %all-gather.9.cloned.1.call-start = ((), (), s32[]{:S(2)}) async-start(), calls=%async_computation.10 | async-start | bytes 4718592 | tf_op jit(solution)/shard_map/all_gather | solution.py:25
  36.2 214.0 %all-gather.7.cloned.1.call-start = ((), (), s32[]{:S(2)}) async-start(), calls=%async_computation.9 | async-start | bytes 4259840 | tf_op jit(solution)/shard_map/all_gather | solution.py:113
  38.5 31.1 %all-to-all-start = ((bf16[8,384,256]{1,2,0:T(8,128)(2,1)}), bf16[8,384,256]{1,2,0:T(8,128)(2,1)S(1)}, u32[]{:S(2)}, u32[]{:S(2)}) async-start(bf16[8,384,256]{1,2,0:T(8,128)(2,1)} %broadcast_in_dim.16), calls=%async_computation | async-start | bytes 3145728 | tf_op jit(solution)/shard_map/all_to_all | solution.py:38
  93.2 1.6 copy-start
  94.8 15.7 %copy-start.2 = (bf16[16,256]{1,0:T(8,128)(2,1)S(1)}, bf16[16,256]{1,0:T(8,128)(2,1)}, u32[]{:S(2)}) copy-start(bf16[16,256]{1,0:T(8,128)(2,1)} %param.15) | copy-start | bytes 24580
  111.4 32.0 %all-to-all-start.3 = ((bf16[64,16,256]{2,1,0:T(8,128)(2,1)}), bf16[64,16,256]{2,1,0:T(8,128)(2,1)S(1)}, u32[]{:S(2)}, u32[]{:S(2)}) async-start(bf16[64,16,256]{2,1,0:T(8,128)(2,1)} %broadcast_in_dim.19), calls=%async_computation.3 | async-start | bytes 1048576 | tf_op jit(solution)/shard_map/all_to_all | solution.py:38
  161.1 8.9 %all-to-all-start.4 = ((f32[8,1,768]{2,1,0:T(1,128)}), f32[8,1,768]{2,1,0:T(1,128)S(1)}, u32[]{:S(2)}, u32[]{:S(2)}) async-start(f32[8,1,768]{2,1,0:T(1,128)} %broadcast_in_dim.20), calls=%async_computation.4 | async-start | bytes 49152 | tf_op jit(solution)/shard_map/all_to_all | solution.py:38
  171.5 24.8 %all-to-all-start.5 = ((bf16[8,384,256]{1,2,0:T(8,128)(2,1)}), bf16[8,384,256]{1,2,0:T(8,128)(2,1)S(1)}, u32[]{:S(2)}, u32[]{:S(2)}) async-start(bf16[8,384,256]{1,2,0:T(8,128)(2,1)} %broadcast_in_dim.21), calls=%async_computation.5 | async-start | bytes 3145728 | tf_op jit(solution)/shard_map/all_to_all | solution.py:38
  287.8 9.0 %all-to-all-start.7 = ((f32[8,1,768]{2,1,0:T(1,128)}), f32[8,1,768]{2,1,0:T(1,128)S(1)}, u32[]{:S(2)}, u32[]{:S(2)}) async-start(f32[8,1,768]{2,1,0:T(1,128)} %broadcast_in_dim.23), calls=%async_computation.7 | async-start | bytes 49152 | tf_op jit(solution)/shard_map/all_to_all | solution.py:38
Sparse Core Ops, SparseCore 0:
  10.4 82.7 all-gather.4
  95.3 69.8 all-gather.8
  168.3 81.8 all-gather.6
where the time goes:
time: 305 us; the launch traced here: 304 us
  waiting for transfers between devices  141 us (46%)
  blocking collectives  87.3 us (29%)
  starting transfers between devices  31.9 us (10%)
  local copies, waits for them, and re-layouts  16.3 us (5%)
  between operations  13.3 us (4%)
  matrix products  9.49 us (3%)
  other arithmetic  5.24 us (2%)
    all_to_all x5, waiting for transfers between devices, sent_to_all(): return lax.all_to_all(copies, axis, split_axis=0, concat_axis=0, tiled=True)  62.7 us
    all_gather x1, waiting for transfers between devices, per_device(): up_collected = lax.all_gather(w_up, FS, axis=0, tiled=True)  53.9 us
    all_to_all x5, starting transfers between devices, sent_to_all(): return lax.all_to_all(copies, axis, split_axis=0, concat_axis=0, tiled=True)  31.8 us
    all_to_all x2, blocking collectives, sent_to_all(): return lax.all_to_all(copies, axis, split_axis=0, concat_axis=0, tiled=True)  30.7 us
    all_to_all x1, blocking collectives, summed_on_arrival(): parts = lax.all_to_all(in_blocks(shard, dim, count), axis, 0, 0, tiled=True)  29.4 us
    all_gather x1, blocking collectives, gather_in_order(): parts = lax.all_gather(parts, axes[k], axis=0, tiled=True)  27.1 us
    all_gather x1, waiting for transfers between devices, in_one_piece(): out, at, done = (lax.all_gather(both, axis, axis=dim, tiled=True), 0, [])  23.6 us
    dot_general x1, matrix products, per_device(): terms = jnp.dot(hidden, down_collected, preferred_element_type=jnp.float32)  6.89 us
  transfers between devices with their start and end apart: 8, of which 7 were waited for; matrix products, arithmetic and copies ran while one was open for 7% of the time, Pallas kernels for 0%

commit v1 on v0

--- a/solution.py
+++ b/solution.py
@@ -110,7 +110,9 @@
     tp_rank = lax.axis_index("tp")
     width_part = tokens.shape[1]
     channel_part = w_value.shape[1]
-    up_collected = lax.all_gather(w_up, FS, axis=0, tiled=True)
+    up_collected = jnp.concatenate(
+        lax.all_to_all(jnp.stack([w_up] * lax.axis_size(FS)), FS, 0, 0), axis=0
+    )
     down_collected = whole_of(w_down, FS, (0, 1), 1)
     features = gather_directly(tokens, "tp", 1)
     values_proj, gate_proj = add_pair(in_one_piece((w_value, w_gate), FS, 0, 1), source=features)

time: 305 us -> 440 us (1.44)
  blocking collectives: 87.3 us -> 196 us
  waiting for transfers between devices: 141 us -> 161 us
    all_gather x1, blocking collectives: 27.1 us -> 115 us  [gather_in_order(): parts = lax.all_gather(parts, axes[k], axis=0, tiled=True)]
    all_gather x1, waiting for transfers between devices: 0.01 us -> 66.4 us  [gather_in_order(): parts = lax.all_gather(parts, axes[k], axis=0, tiled=True)]
    all_gather x1 -> x0, waiting for transfers between devices: 53.9 us -> none  [per_device(): up_collected = lax.all_gather(w_up, FS, axis=0, tiled=True)]
    all_gather x1, waiting for transfers between devices: 23.6 us -> 52 us  [in_one_piece(): out, at, done = (lax.all_gather(both, axis, axis=dim, tiled=True), 0, [])]
    all_to_all x2 -> x3, blocking collectives: 30.7 us -> 55.8 us  [sent_to_all(): return lax.all_to_all(copies, axis, split_axis=0, concat_axis=0, tiled=True)]
    all_to_all x5 -> x4, waiting for transfers between devices: 62.7 us -> 42.6 us  [sent_to_all(): return lax.all_to_all(copies, axis, split_axis=0, concat_axis=0, tiled=True)]
    all_to_all x0 -> x1, starting transfers between devices: none -> 5.79 us  [per_device(): lax.all_to_all(jnp.stack([w_up] * lax.axis_size(FS)), FS, 0, 0)]
    all_to_all x5 -> x4, starting transfers between devices: 31.8 us -> 27.5 us  [sent_to_all(): return lax.all_to_all(copies, axis, split_axis=0, concat_axis=0, tiled=True)]
  transfers between devices with their start and end apart: 8 -> 7, of which waited for: 7 -> 6; matrix products, arithmetic and copies ran while one was open for 7% -> 3% of each run, Pallas kernels for 0% -> 0%
where the time goes in v1:
time: 440 us; the launch traced here: 439 us
  blocking collectives  196 us (45%)
  waiting for transfers between devices  161 us (37%)
  starting transfers between devices  33.3 us (8%)
  local copies, waits for them, and re-layouts  18.4 us (4%)
  between operations  15 us (3%)
  matrix products  9.49 us (2%)
  other arithmetic  5.2 us (1%)
    all_gather x1, blocking collectives, gather_in_order(): parts = lax.all_gather(parts, axes[k], axis=0, tiled=True)  115 us
    all_gather x1, waiting for transfers between devices, gather_in_order(): parts = lax.all_gather(parts, axes[k], axis=0, tiled=True)  66.4 us
    all_to_all x3, blocking collectives, sent_to_all(): return lax.all_to_all(copies, axis, split_axis=0, concat_axis=0, tiled=True)  55.8 us
    all_gather x1, waiting for transfers between devices, in_one_piece(): out, at, done = (lax.all_gather(both, axis, axis=dim, tiled=True), 0, [])  52 us
    all_to_all x4, waiting for transfers between devices, sent_to_all(): return lax.all_to_all(copies, axis, split_axis=0, concat_axis=0, tiled=True)  42.6 us
    all_to_all x4, starting transfers between devices, sent_to_all(): return lax.all_to_all(copies, axis, split_axis=0, concat_axis=0, tiled=True)  27.5 us
    all_to_all x1, blocking collectives, summed_on_arrival(): parts = lax.all_to_all(in_blocks(shard, dim, count), axis, 0, 0, tiled=True)  25.5 us
  transfers between devices with their start and end apart: 7, of which 6 were waited for; matrix products, arithmetic and copies ran while one was open for 3% of the time, Pallas kernels for 0%

profile of v1, /device:TPU:1, one launch (start us, length us, event | category | flops | bytes accessed | tf_op | source)
XLA Modules:
  0.0 438.8 jit_solution(17375884976350513322)
XLA Ops:
  7.4 0.0 all-gather.4.cloned.1.call-start
  7.4 1.3 pad_maximum_fusion
  8.7 0.0 all-gather.4.cloned.1.call-update
  8.7 1.1 copy.53
  9.8 1.3 broadcast_in_dim.16
  11.1 10.3 %all-to-all-start = ((bf16[8,384,256]{1,2,0:T(8,128)(2,1)}), bf16[8,384,256]{1,2,0:T(8,128)(2,1)S(1)}, u32[]{:S(2)}, u32[]{:S(2)}) async-start(bf16[8,384,256]{1,2,0:T(8,128)(2,1)} %broadcast_in_dim.16), calls=%async_computation | async-start | bytes 3145728 | tf_op jit(solution)/shard_map/all_to_all | solution.py:38
  21.4 1.0 fusion.102
  22.5 1.1 fusion.103
  23.6 18.4 %all-to-all-done = bf16[8,384,256]{1,2,0:T(8,128)(2,1)S(1)} async-done(((bf16[8,384,256]{1,2,0:T(8,128)(2,1)}), bf16[8,384,256]{1,2,0:T(8,128)(2,1)S(1)}, u32[]{:S(2)}, u32[]{:S(2)}) %all-to-all-start) | async-done | bytes 1572896 | tf_op jit(solution)/shard_map/all_to_all | solution.py:38
  42.0 52.0 %all-gather.4.cloned.1.call-done = bf16[2048,256]{1,0:T(8,128)(2,1)} async-done(((bf16[32,256]{1,0:T(8,128)(2,1)}), bf16[2048,256]{1,0:T(8,128)(2,1)}) %all-gather.4.cloned.1.call-update) | async-done | bytes 1048592 | tf_op jit(solution)/shard_map/all_gather | solution.py:47
  94.1 0.0 copy-start
  94.1 1.6 fusion.8
  95.7 0.0 copy-done
  95.7 0.0 copy-start.3
  95.7 0.5 fusion.6
  96.2 0.1 copy.55
  96.3 0.7 fusion.106
  97.1 14.2 %all_to_all.48 = f32[8,1,768]{2,1,0:T(1,128)S(1)} all-to-all(f32[8,1,768]{2,1,0:T(1,128)S(1)} %broadcast_in_dim.17), channel_id=1, replica_groups=mesh['fs_0'=8,'fs_1'=8,'tp'=8] {'tp'}, dimensions={0} | all-to-all | bytes 49152 | tf_op jit(solution)/shard_map/all_to_all | solution.py:38
  111.3 0.0 copy-done.3
  111.3 0.8 broadcast_in_dim.19
  112.2 8.6 %all-to-all-start.3 = ((bf16[64,16,256]{2,1,0:T(8,128)(2,1)}), bf16[64,16,256]{2,1,0:T(8,128)(2,1)S(1)}, u32[]{:S(2)}, u32[]{:S(2)}) async-start(bf16[64,16,256]{2,1,0:T(8,128)(2,1)} %broadcast_in_dim.19), calls=%async_computation.3 | async-start | bytes 1048576 | tf_op jit(solution)/shard_map/all_to_all | solution.py:38
  120.8 0.8 dynamic_slice.13
  121.6 0.2 multiply_convert_fusion.3
  121.8 0.1 copy.57
  121.9 16.3 %all-to-all-done.3 = bf16[64,16,256]{2,1,0:T(8,128)(2,1)S(1)} async-done(((bf16[64,16,256]{2,1,0:T(8,128)(2,1)}), bf16[64,16,256]{2,1,0:T(8,128)(2,1)S(1)}, u32[]{:S(2)}, u32[]{:S(2)}) %all-to-all-start.3) | async-done | bytes 524320 | tf_op jit(solution)/shard_map/all_to_all | solution.py:38
  138.2 0.1 broadcast_in_dim.18
  138.2 17.7 %all_to_all.49 = bf16[8,384,128]{1,2,0:T(8,128)(2,1)S(1)} all-to-all(bf16[8,384,128]{1,2,0:T(8,128)(2,1)S(1)} %broadcast_in_dim.18), channel_id=1, replica_groups=mesh['fs_0'=8,'fs_1'=8,'tp'=8] {'tp'}, dimensions={0} | all-to-all | bytes 1572864 | tf_op jit(solution)/shard_map/all_to_all | solution.py:38
  156.0 0.5 fusion.105
  156.5 0.6 broadcast_in_dim.20
  157.1 4.3 all-to-all-start.4
  161.4 0.8 dynamic_slice.14
  162.2 3.9 all-to-all-done.4
  166.1 0.1 multiply_convert_fusion.2
  166.3 0.1 broadcast_in_dim.21
  166.4 0.0 copy-start.1
  166.4 23.8 %all_to_all.50 = bf16[8,384,256]{1,2,0:T(8,128)(2,1)S(1)} all-to-all(bf16[8,384,256]{1,2,0:T(8,128)(2,1)S(1)} %broadcast_in_dim.21), channel_id=1, replica_groups=mesh['fs_0'=8,'fs_1'=8,'tp'=8] {'tp'}, dimensions={0} | all-to-all | bytes 3145728 | tf_op jit(solution)/shard_map/all_to_all | solution.py:38
  190.3 0.0 copy-done.1
  190.3 2.5 stack.2
  192.8 0.0 copy-start.2
  192.8 5.8 %all-to-all-start.6 = ((bf16[64,32,1024]{2,1,0:T(8,128)(2,1)}), bf16[64,32,1024]{2,1,0:T(8,128)(2,1)}, u32[]{:S(2)}, u32[]{:S(2)}) async-start(bf16[64,32,1024]{2,1,0:T(8,128)(2,1)} %stack.2), calls=%async_computation.6 | async-start | bytes 8388608 | tf_op jit(solution)/shard_map/all_to_all | solution.py:114
  198.6 0.0 all-gather.6.cloned.1.call-start
  198.6 0.0 copy-done.2
  198.6 115.0 %all-gather = bf16[8192,32]{0,1:T(8,128)(2,1)S(1)} all-gather(bf16[1024,32]{0,1:T(8,128)(2,1)S(1)} %copy-done.2), channel_id=2, replica_groups=mesh['fs_0'=8,'fs_1'=8,'tp'=8] {'fs_0'}, dimensions={0}, use_global_device_ids=true | all-gather | bytes 589824 | tf_op jit(solution)/shard_map/all_gather | solution.py:25
  313.6 1.1 copy.78
  314.7 0.0 all-gather.6.cloned.1.call-update
  314.8 66.4 %all-gather.6.cloned.1.call-done = bf16[64,1024,32]{1,0,2:T(8,128)(2,1)} async-done(((bf16[8,1024,32]{1,0,2:T(8,128)(2,1)}), bf16[64,1024,32]{1,0,2:T(8,128)(2,1)}) %all-gather.6.cloned.1.call-update) | async-done | bytes 4194320 | tf_op jit(solution)/shard_map/all_gather | solution.py:25
  381.2 6.5 %copy.60 = bf16[8,8,1024,32]{2,3,1,0:T(8,128)(2,1)} copy(bf16[8,8,1024,32]{2,0,1,3:T(8,128)(2,1)} %bitcast.208) | data formatting | bytes 8388608 | tf_op jit(solution)/shard_map/transpose | solution.py:29
  387.6 0.0 all-to-all-done.6
  387.7 6.9 %convolution_convert_fusion = bf16[384,2048]{1,0:T(8,128)(2,1)S(1)} fusion(bf16[1024,2048]{0,1:T(8,128)(2,1)} %bitcast.209, bf16[384,2048]{0,1:T(8,128)(2,1)S(1)} %bitcast.212, bf16[2048,1024]{1,0:T(8,128)(2,1)} %bitcast.44), kind=kOutput, calls=%fused_computation.1 | convolution fusion | flops 3223191552 | bytes 11534336 | tf_op jit(solution)/shard_map/dot_general | solution.py:136
  394.6 0.1 copy.80
  394.7 25.5 %all_to_all.51 = bf16[8,384,256]{2,1,0:T(8,128)(2,1)S(1)} all-to-all(bf16[8,384,256]{2,1,0:T(8,128)(2,1)S(1)} %bitcast.207), channel_id=1, replica_groups=mesh['fs_0'=8,'fs_1'=8,'tp'=8] {'tp'}, dimensions={0} | all-to-all | bytes 3145728 | tf_op jit(solution)/shard_map/all_to_all | solution.py:75
  420.2 0.2 convert_reduce_fusion
  420.4 0.2 copy.63
  420.6 0.2 fusion.72
  420.7 0.6 broadcast_in_dim.23
  421.4 4.3 all-to-all-start.8
  425.7 0.8 dynamic_slice.15
  426.4 3.9 all-to-all-done.8
  430.4 0.2 multiply_convert_fusion.1
  430.6 0.8 copy.65
  (10 shorter events, 0.2 us)
Async XLA Ops:
  7.4 86.7 %all-gather.4.cloned.1.call-start = ((), (), s32[]{:S(2)}) async-start(), calls=%async_computation.9 | async-start | bytes 1064960 | tf_op jit(solution)/shard_map/all_gather | solution.py:47
  11.1 30.9 %all-to-all-start = ((bf16[8,384,256]{1,2,0:T(8,128)(2,1)}), bf16[8,384,256]{1,2,0:T(8,128)(2,1)S(1)}, u32[]{:S(2)}, u32[]{:S(2)}) async-start(bf16[8,384,256]{1,2,0:T(8,128)(2,1)} %broadcast_in_dim.16), calls=%async_computation | async-start | bytes 3145728 | tf_op jit(solution)/shard_map/all_to_all | solution.py:38
  94.1 1.6 copy-start
  95.7 15.7 %copy-start.3 = (bf16[16,256]{1,0:T(8,128)(2,1)S(1)}, bf16[16,256]{1,0:T(8,128)(2,1)}, u32[]{:S(2)}) copy-start(bf16[16,256]{1,0:T(8,128)(2,1)} %param.15) | copy-start | bytes 24580
  112.2 26.0 %all-to-all-start.3 = ((bf16[64,16,256]{2,1,0:T(8,128)(2,1)}), bf16[64,16,256]{2,1,0:T(8,128)(2,1)S(1)}, u32[]{:S(2)}, u32[]{:S(2)}) async-start(bf16[64,16,256]{2,1,0:T(8,128)(2,1)} %broadcast_in_dim.19), calls=%async_computation.3 | async-start | bytes 1048576 | tf_op jit(solution)/shard_map/all_to_all | solution.py:38
  157.1 9.0 %all-to-all-start.4 = ((f32[8,1,768]{2,1,0:T(1,128)}), f32[8,1,768]{2,1,0:T(1,128)S(1)}, u32[]{:S(2)}, u32[]{:S(2)}) async-start(f32[8,1,768]{2,1,0:T(1,128)} %broadcast_in_dim.20), calls=%async_computation.4 | async-start | bytes 49152 | tf_op jit(solution)/shard_map/all_to_all | solution.py:38
  166.4 23.9 %copy-start.1 = (bf16[32,1024]{1,0:T(8,128)(2,1)S(1)}, bf16[32,1024]{1,0:T(8,128)(2,1)}, u32[]{:S(2)}) copy-start(bf16[32,1024]{1,0:T(8,128)(2,1)} %param.17) | copy-start | bytes 196612
  192.8 5.9 %copy-start.2 = (bf16[1024,32]{0,1:T(8,128)(2,1)S(1)}, bf16[1024,32]{0,1:T(8,128)(2,1)}, u32[]{:S(2)}) copy-start(bf16[1024,32]{0,1:T(8,128)(2,1)} %param.18) | copy-start | bytes 196612
  192.8 194.9 %all-to-all-start.6 = ((bf16[64,32,1024]{2,1,0:T(8,128)(2,1)}), bf16[64,32,1024]{2,1,0:T(8,128)(2,1)}, u32[]{:S(2)}, u32[]{:S(2)}) async-start(bf16[64,32,1024]{2,1,0:T(8,128)(2,1)} %stack.2), calls=%async_computation.6 | async-start | bytes 8388608 | tf_op jit(solution)/shard_map/all_to_all | solution.py:114
  198.6 182.6 %all-gather.6.cloned.1.call-start = ((), (), s32[]{:S(2)}) async-start(), calls=%async_computation.10 | async-start | bytes 4718592 | tf_op jit(solution)/shard_map/all_gather | solution.py:25
  421.4 9.0 %all-to-all-start.8 = ((f32[8,1,768]{2,1,0:T(1,128)}), f32[8,1,768]{2,1,0:T(1,128)S(1)}, u32[]{:S(2)}, u32[]{:S(2)}) async-start(f32[8,1,768]{2,1,0:T(1,128)} %broadcast_in_dim.23), calls=%async_computation.8 | async-start | bytes 49152 | tf_op jit(solution)/shard_map/all_to_all | solution.py:38
Sparse Core Ops, SparseCore 0:
  11.2 82.7 all-gather.3
Sparse Core Ops, SparseCore 1:
  314.8 66.3 all-gather.5
